TPU v7x, 512 devices: a whole 4x8x8 slice. The times are simulated.
512 devices in a mesh: sp: 32 (over z, x), tp: 16 (over y, core).
Axes of the slice: x: 4, y: 8, z: 8, core: 2. Of those that a mesh axis runs over, the one named last changes fastest.
Arguments:
- tokens: bfloat16 [32, 3072, 2048], P('sp', 'tp'), may hold values from -100 to 100
- norm_gain: float32 [2048], replicated, may hold values from 0.1 to 1.9
- key_weight: bfloat16 [2048, 1024], P('sp', 'tp'), may hold values from -0.125 to 0.125
- value_weight: bfloat16 [2048, 1024], P('sp', 'tp'), may hold values from -0.125 to 0.125
- cum_gate: float32 [32, 32, 3072], P('sp', None, 'tp'), may hold values from -448 to 0, as said below
- new_gate: float32 [32, 32], P('sp', 'tp'), may hold values from -448 to 0
- new_query: bfloat16 [32, 2048], P('sp', 'tp'), may hold values from -128 to 128
- new_kv: bfloat16 [32, 16, 128], P('sp', 'tp'), may hold values from -4 to 4
Outputs:
- kv_cache: bfloat16 [32, 16, 3072, 128], P('sp', 'tp')
- gate_log_cache: float32 [32, 32, 3072], P('sp', 'tp')
- read_out: bfloat16 [32, 2048], P('sp', 'tp')
Inputs may be any that keep to these rules, and one draw needn't show every extreme that they name: Along positions cum_gate never rises; new_gate is at most the last position's value of its prompt and head.
All inputs are finite; a program needn't handle non-finite values.
Results may differ from a plain program's by a relative error of at most 0.0071.
Values may be sent and summed in bfloat16 or wider, within the bound.
No kernel may reach another device: no remote copies, remote signals or barrier semaphores. Data moves between devices by JAX's collectives and lax.ppermute only.
A program may use at most 64 MiB of HBM per device.

v0:
```python
import functools
import math

import jax
import jax.numpy as jnp
from jax import lax
from jax.experimental import pallas as pl
from jax.experimental.pallas import tpu as pltpu
from jax.sharding import Mesh, PartitionSpec as P

HEAD = 64
WIDE = 2 * HEAD
RING = 8
POS = 192
AHEAD = [(2 * y + c, 2 * ((y + 1 - 2 * c) % RING) + c) for y in range(RING) for c in (0, 1)]
SWAP = [(0, 1), (1, 0)]
KINDS = (((0, 0), (1, 0), (1, 1), (2, 0), (2, 1)), ((3, 0), (3, 1)), ((4, 0),))
VMEM = pl.BlockSpec(memory_space=pltpu.VMEM)
LIMIT = pltpu.CompilerParams(vmem_limit_bytes=16 * 2**20)


def on_chip(array):
    return pltpu.with_memory_space_constraint(array, pltpu.VMEM)


def project_body(count, *refs):
    rows = refs[:count]
    gain, mine, other = refs[count : count + 3]
    before = refs[count + 3 : -2]
    out_mine, out_other = refs[-2:]
    held = 0
    for ref in before:
        out_other[held : held + ref.shape[0], :] = ref[...]
        held += ref.shape[0]
    for k, ref in enumerate(rows):
        wide = ref[...].astype(jnp.float32)
        inv_rms = lax.rsqrt(jnp.mean(wide * wide, axis=1, keepdims=True) + 1e-06)
        scaled = (wide * gain[...]).astype(jnp.bfloat16)
        for weight, out, skip in ((mine, out_mine, 0), (other, out_other, held)):
            product = jnp.dot(scaled, weight[...], preferred_element_type=jnp.float32)
            at = skip + k * POS
            out[at : at + POS, :] = (product * inv_rms).astype(jnp.bfloat16)


def project(rows, gain, weights, before=()):
    height = POS * len(rows)
    held = sum(b.shape[0] for b in before)
    return pl.pallas_call(
        functools.partial(project_body, len(rows)),
        out_shape=(
            pltpu.VMEM((height, WIDE), jnp.bfloat16),
            pltpu.VMEM((held + height, WIDE), jnp.bfloat16),
        ),
        in_specs=[VMEM] * (len(rows) + 3 + len(before)),
        out_specs=(VMEM, VMEM),
        compiler_params=LIMIT,
        cost_estimate=pl.CostEstimate(
            flops=height * 2048 * 512, bytes_accessed=height * 2048 * 2, transcendentals=0
        ),
    )(*rows, gain, *weights, *before)


def finish_body(gates, small, *refs):
    pieces = refs[:4]
    cache, gate_out, read, sems = refs[4:]
    at, core = lax.axis_index("y"), lax.axis_index("c")
    way = 1 - 2 * core
    blocks, copies = [], []
    kinds = KINDS + (sum(KINDS, ()),)
    for k, ref in enumerate(pieces):
        partner = k // 3
        sign = way * (2 * partner - 1)
        for row, (hops, crossed) in enumerate(kinds[k]):
            side = (core + partner + crossed) % 2
            place = (at + sign * hops + RING) % RING * 2 + side
            block = ref.at[row * POS : (row + 1) * POS, :]
            start = pl.multiple_of(place * POS, POS)
            copy = pltpu.make_async_copy(block, cache.at[pl.ds(start, POS), :], sems.at[len(copies)])
            copy.start()
            copies.append(copy)
            blocks.append((block, place))
    gate_out[...] = jnp.concatenate([gates[p] for p in range(2 * RING)], axis=1)
    factor = 1.0 / math.sqrt(HEAD)
    lane = lax.broadcasted_iota(jnp.int32, (2, WIDE), 1)
    head = lax.broadcasted_iota(jnp.int32, (2, WIDE), 0)
    both = jnp.broadcast_to(small[0:1, :], (2, WIDE))
    new = jnp.broadcast_to(small[1:2, :], (2, WIDE))
    fresh = jnp.sum(jnp.where(lane == head, small[2:3, :], 0.0), axis=1, keepdims=True)
    keyed = jnp.where(lane < HEAD, jnp.where(head == 0, both, pltpu.roll(both, HEAD, 1)), 0.0)
    own = jnp.sum(keyed * new, axis=1, keepdims=True) * factor
    query = keyed.astype(jnp.bfloat16)
    scores = []
    for block, place in blocks:
        raw = lax.dot_general(
            query, block[...], (((1,), (1,)), ((), ())), preferred_element_type=jnp.float32
        )
        scores.append(raw * factor + fresh - gates[place])
    peak = functools.reduce(jnp.maximum, scores)
    top = jnp.maximum(jnp.max(peak, axis=1, keepdims=True), own)
    own_factor = jnp.exp(own - top)
    total = jnp.zeros((2, POS), jnp.float32)
    numer = own_factor * new
    for (block, _), score in zip(blocks, scores):
        expo = jnp.exp(score - top)
        total += expo
        numer += jnp.dot(expo.astype(jnp.bfloat16), block[...], preferred_element_type=jnp.float32)
    result = numer / (jnp.sum(total, axis=1, keepdims=True) + own_factor)
    shifted = pltpu.roll(result, HEAD, 1)
    read[...] = jnp.where(lane[:1] < HEAD, shifted[:1], result[1:]).astype(jnp.bfloat16)
    for copy in copies:
        copy.wait()


def finish(gates, small, pieces):
    return pl.pallas_call(
        finish_body,
        out_shape=(
            jax.ShapeDtypeStruct((2 * RING * POS, WIDE), jnp.bfloat16),
            jax.ShapeDtypeStruct((2, 2 * RING * POS), jnp.float32),
            jax.ShapeDtypeStruct((1, WIDE), jnp.bfloat16),
        ),
        in_specs=[VMEM] * 6,
        out_specs=(pl.BlockSpec(memory_space=pl.ANY), VMEM, VMEM),
        scratch_shapes=[pltpu.SemaphoreType.DMA((2 * RING,))],
        compiler_params=LIMIT,
    )(on_chip(gates), on_chip(small), *[on_chip(p) for p in pieces])


def per_device(tokens, norm_gain, key_weight, value_weight, cum_gate, new_gate, new_query, new_kv):
    block = tokens[0]
    tp = ("y", "c")
    ahead = [lax.ppermute(block, tp, AHEAD)]

    local = jnp.concatenate([key_weight, value_weight], axis=1)
    spread = jnp.broadcast_to(local[None], (32,) + local.shape)
    gain = jnp.broadcast_to(norm_gain[None], (1, 2048))
    small = jnp.concatenate(
        [
            new_query.astype(jnp.float32),
            new_kv[0].astype(jnp.float32),
            jnp.pad(new_gate, ((0, 0), (0, WIDE - 2))),
        ],
        axis=0,
    )
    gate_parts = cum_gate[0].reshape(2 * RING, 2, POS)
    fellow = lax.ppermute(block, "c", SWAP)
    fellow, gain, small, gate_parts, spread = lax.optimization_barrier(
        (fellow, gain, small, gate_parts, spread)
    )
    crossed = [lax.ppermute(fellow, tp, AHEAD)]
    gathered = lax.all_to_all(spread, ("z", "x"), 0, 0, tiled=True)
    mine = gathered.reshape(2048, WIDE)
    weights = [on_chip(mine), on_chip(lax.ppermute(mine, "c", SWAP))]

    for step in (2, 3, 4):
        ahead.append(lax.ppermute(ahead[-1], tp, AHEAD))
        if step < 4:
            crossed.append(lax.ppermute(crossed[-1], tp, AHEAD))
    gates = lax.all_to_all(gate_parts, tp, split_axis=0, concat_axis=0, tiled=True)

    gain = on_chip(gain)
    first = [block] + [on_chip(r) for r in (ahead[0], crossed[0], ahead[1], crossed[1])]
    kept0, other0 = project(first, gain, weights)
    kept1, other1 = project([on_chip(ahead[2]), on_chip(crossed[2])], gain, weights)
    before = [on_chip(other0), on_chip(other1)]
    kept2, others = project([on_chip(ahead[3])], gain, weights, before)
    swapped = lax.ppermute(others, "c", SWAP)
    cache, gate_out, read = finish(gates, small, (kept0, kept1, kept2, swapped))
    return (cache[None, None], gate_out[None], read)


def solution(mesh):
    fine = Mesh(mesh.devices.reshape(8, 4, 8, 2), ("z", "x", "y", "c"))
    sp, tp = ("z", "x"), ("y", "c")
    in_specs = (
        P(sp, tp, None),
        P(),
        P(sp, tp),
        P(sp, tp),
        P(sp, None, tp),
        P(sp, tp),
        P(sp, tp),
        P(sp, tp, None),
    )
    out_specs = (P(sp, tp, None, None), P(sp, tp, None), P(sp, tp))
    return jax.shard_map(
        per_device, mesh=fine, in_specs=in_specs, out_specs=out_specs, check_vma=False
    )
```

profile of v0, /device:TPU:1, one launch (start us, length us, event | category | flops | bytes accessed | tf_op | source)
XLA Modules:
  0.0 95.8 jit_solution(2742791443497786160)
XLA Ops:
  0.6 0.0 copy-start.6
  0.6 8.7 %collective-permute-start = (bf16[192,2048]{1,0:T(8,128)(2,1)}, bf16[192,2048]{1,0:T(8,128)(2,1)S(1)}, u32[]{:S(2)}, u32[]{:S(2)}) collective-permute-start(bf16[192,2048]{1,0:T(8,128)(2,1)} %bitcast.12), channel_id=1, source_target_pairs={{0,1},{1,0},{2,3},{3,2},{4,5},{5,4},{6,7},{7,6},{8,9},{9,8},{10,11... | collective-permute-start | bytes 2359304 | tf_op jit(solution)/shard_map/ppermute | solution.py:146
  9.4 1.9 %collective-permute-start.1 = (bf16[192,2048]{1,0:T(8,128)(2,1)}, bf16[192,2048]{1,0:T(8,128)(2,1)S(1)}, u32[]{:S(2)}, u32[]{:S(2)}) collective-permute-start(bf16[192,2048]{1,0:T(8,128)(2,1)} %bitcast.13), channel_id=1, source_target_pairs={{0,2},{1,15},{2,4},{3,1},{4,6},{5,3},{6,8},{7,5},{8,10},{9,7},{10,... | collective-permute-start | bytes 2359304 | tf_op jit(solution)/shard_map/ppermute | solution.py:132
  11.3 0.0 copy-done.6
  11.3 0.0 copy-start.7
  11.4 0.0 copy-start.2
  11.4 0.0 copy-start.3
  11.4 0.8 reshape_squeeze.3
  12.2 0.0 copy-done.7
  12.2 0.0 copy-start.4
  12.2 0.6 copy-done.4
  12.9 0.0 copy-done.2
  12.9 0.0 copy-done.3
  12.9 0.1 pad_maximum_fusion
  13.0 0.0 collective-permute-done
  13.0 0.0 copy-start.5
  13.0 0.9 copy-done.5
  13.9 0.0 copy-start
  13.9 0.9 broadcast_in_dim.16
  14.8 0.0 copy-start.1
  14.8 2.0 %collective-permute-start.2 = (bf16[192,2048]{1,0:T(8,128)(2,1)}, bf16[192,2048]{1,0:T(8,128)(2,1)S(1)}, u32[]{:S(2)}, u32[]{:S(2)}) collective-permute-start(bf16[192,2048]{1,0:T(8,128)(2,1)} %copy-done.5), channel_id=1, source_target_pairs={{0,2},{1,15},{2,4},{3,1},{4,6},{5,3},{6,8},{7,5},{8,10},{9,7},{10,... | collective-permute-start | bytes 2359304 | tf_op jit(solution)/shard_map/ppermute | solution.py:150
  16.8 5.8 %collective-permute-done.1.refs_1_ = bf16[192,2048]{1,0:T(8,128)(2,1)S(1)} collective-permute-done((bf16[192,2048]{1,0:T(8,128)(2,1)}, bf16[192,2048]{1,0:T(8,128)(2,1)S(1)}, u32[]{:S(2)}, u32[]{:S(2)}) %collective-permute-start.1) | collective-permute-done | bytes 786464 | tf_op jit(solution)/shard_map/ppermute | solution.py:132
  22.6 2.8 %collective-permute-start.3 = (bf16[192,2048]{1,0:T(8,128)(2,1)S(1)}, bf16[192,2048]{1,0:T(8,128)(2,1)}, u32[]{:S(2)}, u32[]{:S(2)}) collective-permute-start(bf16[192,2048]{1,0:T(8,128)(2,1)S(1)} %collective-permute-done.1.refs_1_), channel_id=1, source_target_pairs={{0,2},{1,15},{2,4},{3,1},{4,6},{5,3},{6,8},{7,5},{8,10},{9,7},{10,... | collective-permute-start | bytes 2359304 | tf_op jit(solution)/shard_map/ppermute | solution.py:156
  25.5 10.7 %all-to-all-start.1 = ((bf16[32,64,128]{2,1,0:T(8,128)(2,1)}), bf16[32,64,128]{2,1,0:T(8,128)(2,1)S(1)}, u32[]{:S(2)}, u32[]{:S(2)}) async-start(bf16[32,64,128]{2,1,0:T(8,128)(2,1)} %broadcast_in_dim.16), calls=%async_computation.1 | async-start | bytes 1048576 | tf_op jit(solution)/shard_map/all_to_all | solution.py:151
  36.2 0.0 collective-permute-done.2.refs_2_
  36.2 2.1 %collective-permute-start.4 = (bf16[192,2048]{1,0:T(8,128)(2,1)S(1)}, bf16[192,2048]{1,0:T(8,128)(2,1)}, u32[]{:S(2)}, u32[]{:S(2)}) collective-permute-start(bf16[192,2048]{1,0:T(8,128)(2,1)S(1)} %collective-permute-done.2.refs_2_), channel_id=1, source_target_pairs={{0,2},{1,15},{2,4},{3,1},{4,6},{5,3},{6,8},{7,5},{8,10},{9,7},{10,... | collective-permute-start | bytes 2359304 | tf_op jit(solution)/shard_map/ppermute | solution.py:158
  38.3 1.3 %collective-permute-done.3.refs_3_ = bf16[192,2048]{1,0:T(8,128)(2,1)} collective-permute-done((bf16[192,2048]{1,0:T(8,128)(2,1)S(1)}, bf16[192,2048]{1,0:T(8,128)(2,1)}, u32[]{:S(2)}, u32[]{:S(2)}) %collective-permute-start.3) | collective-permute-done | bytes 786464 | tf_op jit(solution)/shard_map/ppermute | solution.py:156
  39.6 2.8 %collective-permute-start.6 = (bf16[192,2048]{1,0:T(8,128)(2,1)}, bf16[192,2048]{1,0:T(8,128)(2,1)}, u32[]{:S(2)}, u32[]{:S(2)}) collective-permute-start(bf16[192,2048]{1,0:T(8,128)(2,1)} %collective-permute-done.3.refs_3_), channel_id=1, source_target_pairs={{0,2},{1,15},{2,4},{3,1},{4,6},{5,3},{6,8},{7,5},{8,10},{9,7},{10,... | collective-permute-start | bytes 2359304 | tf_op jit(solution)/shard_map/ppermute | solution.py:156
  42.4 6.9 %collective-permute-done.4.refs_4_ = bf16[192,2048]{1,0:T(8,128)(2,1)} collective-permute-done((bf16[192,2048]{1,0:T(8,128)(2,1)S(1)}, bf16[192,2048]{1,0:T(8,128)(2,1)}, u32[]{:S(2)}, u32[]{:S(2)}) %collective-permute-start.4) | collective-permute-done | bytes 786464 | tf_op jit(solution)/shard_map/ppermute | solution.py:158
  49.4 3.2 %collective-permute-start.7 = (bf16[192,2048]{1,0:T(8,128)(2,1)}, bf16[192,2048]{1,0:T(8,128)(2,1)}, u32[]{:S(2)}, u32[]{:S(2)}) collective-permute-start(bf16[192,2048]{1,0:T(8,128)(2,1)} %collective-permute-done.4.refs_4_), channel_id=1, source_target_pairs={{0,2},{1,15},{2,4},{3,1},{4,6},{5,3},{6,8},{7,5},{8,10},{9,7},{10,... | collective-permute-start | bytes 2359304 | tf_op jit(solution)/shard_map/ppermute | solution.py:158
  52.5 5.3 %collective-permute-done.6.refs_0_ = bf16[192,2048]{1,0:T(8,128)(2,1)} collective-permute-done((bf16[192,2048]{1,0:T(8,128)(2,1)}, bf16[192,2048]{1,0:T(8,128)(2,1)}, u32[]{:S(2)}, u32[]{:S(2)}) %collective-permute-start.6) | collective-permute-done | bytes 786464 | tf_op jit(solution)/shard_map/ppermute | solution.py:156
  57.8 3.0 %collective-permute-start.8 = (bf16[192,2048]{1,0:T(8,128)(2,1)}, bf16[192,2048]{1,0:T(8,128)(2,1)}, u32[]{:S(2)}, u32[]{:S(2)}) collective-permute-start(bf16[192,2048]{1,0:T(8,128)(2,1)} %collective-permute-done.6.refs_0_), channel_id=1, source_target_pairs={{0,2},{1,15},{2,4},{3,1},{4,6},{5,3},{6,8},{7,5},{8,10},{9,7},{10,... | collective-permute-start | bytes 2359304 | tf_op jit(solution)/shard_map/ppermute | solution.py:156
  60.8 0.0 all-to-all-done.1
  60.8 1.9 %collective-permute-start.5 = (bf16[2048,128]{1,0:T(8,128)(2,1)S(1)}, bf16[2048,128]{1,0:T(8,128)(2,1)S(1)}, u32[]{:S(2)}, u32[]{:S(2)}) collective-permute-start(bf16[2048,128]{1,0:T(8,128)(2,1)S(1)} %bitcast.8), channel_id=1, source_target_pairs={{0,1},{1,0},{2,3},{3,2},{4,5},{5,4},{6,7},{7,6},{8,9},{9,8},{10,11... | collective-permute-start | bytes 1572872 | tf_op jit(solution)/shard_map/ppermute | solution.py:153
  62.7 1.9 %collective-permute-done.5.refs_7_.refs_4_.refs_3_ = bf16[2048,128]{1,0:T(8,128)(2,1)S(1)} collective-permute-done((bf16[2048,128]{1,0:T(8,128)(2,1)S(1)}, bf16[2048,128]{1,0:T(8,128)(2,1)S(1)}, u32[]{:S(2)}, u32[]{:S(2)}) %collective-permute-start.5) | collective-permute-done | bytes 524320 | tf_op jit(solution)/shard_map/ppermute | solution.py:153
  64.6 0.0 copy-done
  64.6 0.0 copy-done.1
  64.6 3.8 %shard_map.103 = (bf16[960,128]{1,0:T(8,128)(2,1)S(1)}, bf16[960,128]{1,0:T(8,128)(2,1)S(1)}) custom-call(bf16[192,2048]{1,0:T(8,128)(2,1)S(1)} %bitcast.14, bf16[192,2048]{1,0:T(8,128)(2,1)S(1)} %collective-permute-done.1.refs_1_, bf16[192,2048]{1,0:T(8,128)(2,1)S(1)} %collective-permute-done.2.refs_2_, bf16[192,2048]{1,0:T(8,128)(2,1)} %collective-permute-done.3.refs_3_, ...), custom_call_target="tpu_custom_call" | custom-call | flops 1006632960 | bytes 3932160 | tf_op jit(solution)/shard_map/pallas_call | solution.py:48
  68.4 0.0 collective-permute-done.7.refs_1_
  68.4 2.4 %shard_map.104 = (bf16[384,128]{1,0:T(8,128)(2,1)S(1)}, bf16[384,128]{1,0:T(8,128)(2,1)S(1)}) custom-call(bf16[192,2048]{1,0:T(8,128)(2,1)} %collective-permute-done.6.refs_0_, bf16[192,2048]{1,0:T(8,128)(2,1)} %collective-permute-done.7.refs_1_, f32[1,2048]{1,0:T(1,128)S(1)} %bitcast.16, bf16[2048,128]{1,0:T(8,128)(2,1)S(1)} %bitcast.10, ...), custom_call_target="tpu_custom_call" | custom-call | flops 402653184 | bytes 1572864 | tf_op jit(solution)/shard_map/pallas_call | solution.py:48
  70.9 3.8 %collective-permute-done.8.refs_0_ = bf16[192,2048]{1,0:T(8,128)(2,1)} collective-permute-done((bf16[192,2048]{1,0:T(8,128)(2,1)}, bf16[192,2048]{1,0:T(8,128)(2,1)}, u32[]{:S(2)}, u32[]{:S(2)}) %collective-permute-start.8) | collective-permute-done | bytes 786464 | tf_op jit(solution)/shard_map/ppermute | solution.py:156
  74.6 1.8 %shard_map.105 = (bf16[192,128]{1,0:T(8,128)(2,1)S(1)}, bf16[1536,128]{1,0:T(8,128)(2,1)S(1)}) custom-call(bf16[192,2048]{1,0:T(8,128)(2,1)} %collective-permute-done.8.refs_0_, f32[1,2048]{1,0:T(1,128)S(1)} %bitcast.17, bf16[2048,128]{1,0:T(8,128)(2,1)S(1)} %bitcast.11, bf16[2048,128]{1,0:T(8,128)(2,1)S(1)} %collective-permute-done.5.refs_7_.refs_4_.refs_3_, ...), custom_call_target="tpu_custom_call" | custom-call | flops 201326592 | bytes 786432 | tf_op jit(solution)/shard_map/pallas_call | solution.py:48
  76.4 2.7 %collective-permute-start.9 = (bf16[1536,128]{1,0:T(8,128)(2,1)S(1)}, bf16[1536,128]{1,0:T(8,128)(2,1)S(1)}, u32[]{:S(2)}, u32[]{:S(2)}) collective-permute-start(bf16[1536,128]{1,0:T(8,128)(2,1)S(1)} %get-tuple-element.27), channel_id=1, source_target_pairs={{0,1},{1,0},{2,3},{3,2},{4,5},{5,4},{6,7},{7,6},{8,9},{9,8},{10,11... | collective-permute-start | bytes 1179656 | tf_op jit(solution)/shard_map/ppermute | solution.py:167
  79.1 14.0 %all_to_all.10.gates = f32[16,2,192]{2,1,0:T(2,128)S(1)} all-to-all(f32[16,2,192]{2,1,0:T(2,128)S(1)} %reshape_squeeze.3), channel_id=1, replica_groups=mesh['z'=8,'x'=4,'y'=8,'c'=2] {'y','c'}, dimensions={0} | all-to-all | bytes 49152 | tf_op jit(solution)/shard_map/all_to_all | solution.py:159
  93.1 0.0 collective-permute-done.9.refs_3_
  93.1 2.7 %shard_map.106 = (bf16[3072,128]{1,0:T(8,128)(2,1)}, f32[2,3072]{1,0:T(2,128)}, bf16[1,128]{1,0:T(2,128)(2,1)}) custom-call(f32[16,2,192]{2,1,0:T(2,128)S(1)} %all_to_all.10.gates, f32[3,128]{1,0:T(4,128)S(1)} %select_maximum_fusion.small, bf16[960,128]{1,0:T(8,128)(2,1)S(1)} %get-tuple-element.22.refs_0_, bf16[384,128]{1,0:T(8,128)(2,1)S(1)} %get-tuple-element.23.refs_1_, ...), custom_call_target="tpu_custom_call" | custom-call | tf_op jit(solution)/shard_map/pallas_call | solution.py:115
  (3 shorter events, 0.0 us)
Async XLA Ops:
  0.6 10.7 %copy-start.6 = (bf16[1,128]{1,0:T(2,128)(2,1)S(1)}, bf16[1,128]{1,0:T(2,128)(2,1)}, u32[]{:S(2)}) copy-start(bf16[1,128]{1,0:T(2,128)(2,1)} %param.14) | copy-start | bytes 772
  0.6 12.3 %collective-permute-start = (bf16[192,2048]{1,0:T(8,128)(2,1)}, bf16[192,2048]{1,0:T(8,128)(2,1)S(1)}, u32[]{:S(2)}, u32[]{:S(2)}) collective-permute-start(bf16[192,2048]{1,0:T(8,128)(2,1)} %bitcast.12), channel_id=1, source_target_pairs={{0,1},{1,0},{2,3},{3,2},{4,5},{5,4},{6,7},{7,6},{8,9},{9,8},{10,11... | collective-permute-start | bytes 2359304 | tf_op jit(solution)/shard_map/ppermute | solution.py:146
  9.4 13.2 %collective-permute-start.1 = (bf16[192,2048]{1,0:T(8,128)(2,1)}, bf16[192,2048]{1,0:T(8,128)(2,1)S(1)}, u32[]{:S(2)}, u32[]{:S(2)}) collective-permute-start(bf16[192,2048]{1,0:T(8,128)(2,1)} %bitcast.13), channel_id=1, source_target_pairs={{0,2},{1,15},{2,4},{3,1},{4,6},{5,3},{6,8},{7,5},{8,10},{9,7},{10,... | collective-permute-start | bytes 2359304 | tf_op jit(solution)/shard_map/ppermute | solution.py:132
  11.3 0.8 copy-start.7
  11.4 1.5 %copy-start.2 = (bf16[64,64]{1,0:T(8,128)(2,1)S(1)}, bf16[64,64]{1,0:T(8,128)(2,1)}, u32[]{:S(2)}) copy-start(bf16[64,64]{1,0:T(8,128)(2,1)} %param.11) | copy-start | bytes 24580
  11.4 1.5 %copy-start.3 = (bf16[64,64]{1,0:T(8,128)(2,1)S(1)}, bf16[64,64]{1,0:T(8,128)(2,1)}, u32[]{:S(2)}) copy-start(bf16[64,64]{1,0:T(8,128)(2,1)} %param.10) | copy-start | bytes 24580
  12.2 0.7 copy-start.4
  13.0 0.9 copy-start.5
  13.9 50.7 %copy-start = (bf16[1,192,2048]{2,1,0:T(8,128)(2,1)S(1)}, bf16[1,192,2048]{2,1,0:T(8,128)(2,1)}, u32[]{:S(2)}) copy-start(bf16[1,192,2048]{2,1,0:T(8,128)(2,1)} %param.8) | copy-start | bytes 2359300
  14.8 49.8 %copy-start.1 = (f32[2048]{0:T(1024)S(1)}, f32[2048]{0:T(1024)}, u32[]{:S(2)}) copy-start(f32[2048]{0:T(1024)} %param.9) | copy-start | bytes 24580
  14.8 21.4 %collective-permute-start.2 = (bf16[192,2048]{1,0:T(8,128)(2,1)}, bf16[192,2048]{1,0:T(8,128)(2,1)S(1)}, u32[]{:S(2)}, u32[]{:S(2)}) collective-permute-start(bf16[192,2048]{1,0:T(8,128)(2,1)} %copy-done.5), channel_id=1, source_target_pairs={{0,2},{1,15},{2,4},{3,1},{4,6},{5,3},{6,8},{7,5},{8,10},{9,7},{10,... | collective-permute-start | bytes 2359304 | tf_op jit(solution)/shard_map/ppermute | solution.py:150
  22.6 17.0 %collective-permute-start.3 = (bf16[192,2048]{1,0:T(8,128)(2,1)S(1)}, bf16[192,2048]{1,0:T(8,128)(2,1)}, u32[]{:S(2)}, u32[]{:S(2)}) collective-permute-start(bf16[192,2048]{1,0:T(8,128)(2,1)S(1)} %collective-permute-done.1.refs_1_), channel_id=1, source_target_pairs={{0,2},{1,15},{2,4},{3,1},{4,6},{5,3},{6,8},{7,5},{8,10},{9,7},{10,... | collective-permute-start | bytes 2359304 | tf_op jit(solution)/shard_map/ppermute | solution.py:156
  25.5 35.3 %all-to-all-start.1 = ((bf16[32,64,128]{2,1,0:T(8,128)(2,1)}), bf16[32,64,128]{2,1,0:T(8,128)(2,1)S(1)}, u32[]{:S(2)}, u32[]{:S(2)}) async-start(bf16[32,64,128]{2,1,0:T(8,128)(2,1)} %broadcast_in_dim.16), calls=%async_computation.1 | async-start | bytes 1048576 | tf_op jit(solution)/shard_map/all_to_all | solution.py:151
  36.2 13.1 %collective-permute-start.4 = (bf16[192,2048]{1,0:T(8,128)(2,1)S(1)}, bf16[192,2048]{1,0:T(8,128)(2,1)}, u32[]{:S(2)}, u32[]{:S(2)}) collective-permute-start(bf16[192,2048]{1,0:T(8,128)(2,1)S(1)} %collective-permute-done.2.refs_2_), channel_id=1, source_target_pairs={{0,2},{1,15},{2,4},{3,1},{4,6},{5,3},{6,8},{7,5},{8,10},{9,7},{10,... | collective-permute-start | bytes 2359304 | tf_op jit(solution)/shard_map/ppermute | solution.py:158
  39.6 18.2 %collective-permute-start.6 = (bf16[192,2048]{1,0:T(8,128)(2,1)}, bf16[192,2048]{1,0:T(8,128)(2,1)}, u32[]{:S(2)}, u32[]{:S(2)}) collective-permute-start(bf16[192,2048]{1,0:T(8,128)(2,1)} %collective-permute-done.3.refs_3_), channel_id=1, source_target_pairs={{0,2},{1,15},{2,4},{3,1},{4,6},{5,3},{6,8},{7,5},{8,10},{9,7},{10,... | collective-permute-start | bytes 2359304 | tf_op jit(solution)/shard_map/ppermute | solution.py:156
  49.4 19.1 %collective-permute-start.7 = (bf16[192,2048]{1,0:T(8,128)(2,1)}, bf16[192,2048]{1,0:T(8,128)(2,1)}, u32[]{:S(2)}, u32[]{:S(2)}) collective-permute-start(bf16[192,2048]{1,0:T(8,128)(2,1)} %collective-permute-done.4.refs_4_), channel_id=1, source_target_pairs={{0,2},{1,15},{2,4},{3,1},{4,6},{5,3},{6,8},{7,5},{8,10},{9,7},{10,... | collective-permute-start | bytes 2359304 | tf_op jit(solution)/shard_map/ppermute | solution.py:158
  57.8 16.9 %collective-permute-start.8 = (bf16[192,2048]{1,0:T(8,128)(2,1)}, bf16[192,2048]{1,0:T(8,128)(2,1)}, u32[]{:S(2)}, u32[]{:S(2)}) collective-permute-start(bf16[192,2048]{1,0:T(8,128)(2,1)} %collective-permute-done.6.refs_0_), channel_id=1, source_target_pairs={{0,2},{1,15},{2,4},{3,1},{4,6},{5,3},{6,8},{7,5},{8,10},{9,7},{10,... | collective-permute-start | bytes 2359304 | tf_op jit(solution)/shard_map/ppermute | solution.py:156
  60.8 3.8 %collective-permute-start.5 = (bf16[2048,128]{1,0:T(8,128)(2,1)S(1)}, bf16[2048,128]{1,0:T(8,128)(2,1)S(1)}, u32[]{:S(2)}, u32[]{:S(2)}) collective-permute-start(bf16[2048,128]{1,0:T(8,128)(2,1)S(1)} %bitcast.8), channel_id=1, source_target_pairs={{0,1},{1,0},{2,3},{3,2},{4,5},{5,4},{6,7},{7,6},{8,9},{9,8},{10,11... | collective-permute-start | bytes 1572872 | tf_op jit(solution)/shard_map/ppermute | solution.py:153
  76.4 16.7 %collective-permute-start.9 = (bf16[1536,128]{1,0:T(8,128)(2,1)S(1)}, bf16[1536,128]{1,0:T(8,128)(2,1)S(1)}, u32[]{:S(2)}, u32[]{:S(2)}) collective-permute-start(bf16[1536,128]{1,0:T(8,128)(2,1)S(1)} %get-tuple-element.27), channel_id=1, source_target_pairs={{0,1},{1,0},{2,3},{3,2},{4,5},{5,4},{6,7},{7,6},{8,9},{9,8},{10,11... | collective-permute-start | bytes 1179656 | tf_op jit(solution)/shard_map/ppermute | solution.py:167
where the time goes:
time: 96.5 us; the launch traced here: 95.8 us
  starting transfers between devices  41.8 us (43%)
  waiting for transfers between devices  25 us (26%)
  blocking collectives  14 us (15%)
  Pallas kernels  10.8 us (11%)
  local copies, waits for them, and re-layouts  3.26 us (3%)
    all_to_all x1, blocking collectives, per_device(): lax.all_to_all(gate_parts, tp, split_axis=0, concat_axis=0, tiled=True)  14 us
    all_to_all x1, starting transfers between devices, per_device(): gathered = lax.all_to_all(spread, ('z', 'x'), 0, 0, tiled=True)  10.7 us
    ppermute x3, waiting for transfers between devices, per_device(): ahead.append(lax.ppermute(ahead[-1], tp, AHEAD))  10.3 us
    ppermute x1, starting transfers between devices, per_device(): fellow = lax.ppermute(block, 'c', SWAP)  8.75 us
    ppermute x3, starting transfers between devices, per_device(): ahead.append(lax.ppermute(ahead[-1], tp, AHEAD))  8.62 us
    pallas_call x3, Pallas kernels, project(): pl.pallas_call(functools.partial(project_body, len(rows)), out_shape=(plt...  8.04 us
    ppermute x2, waiting for transfers between devices, per_device(): crossed.append(lax.ppermute(crossed[-1], tp, AHEAD))  6.93 us
    ppermute x1, waiting for transfers between devices, per_device(): ahead = [lax.ppermute(block, tp, AHEAD)]  5.82 us
  transfers between devices with their start and end apart: 11, of which 6 were waited for; matrix products, arithmetic and copies ran while one was open for 2% of the time, Pallas kernels for 7%

commit v1 on v0

v1 whole, which is shorter than its diff:
```python
import functools
import math

import jax
import jax.numpy as jnp
from jax import lax
from jax.experimental import pallas as pl
from jax.experimental.pallas import tpu as pltpu
from jax.sharding import Mesh, PartitionSpec as P

HEAD = 64
WIDE = 2 * HEAD
RING = 8
POS = 192
AHEAD = [(2 * y + c, 2 * ((y + 1 - 2 * c) % RING) + c) for y in range(RING) for c in (0, 1)]
SWAP = [(0, 1), (1, 0)]
FACTOR = 1.0 / math.sqrt(HEAD)
EARLY = ((0, 0), (1, 0), (1, 1), (2, 0), (2, 1), (3, 0), (3, 1))
LATE = ((4, 0),)
VMEM = pl.BlockSpec(memory_space=pltpu.VMEM)
ANY = pl.BlockSpec(memory_space=pl.ANY)
LIMIT = pltpu.CompilerParams(vmem_limit_bytes=16 * 2**20)


def on_chip(array):
    return pltpu.with_memory_space_constraint(array, pltpu.VMEM)


def project_block(rows, gain, mine, other, out_mine, out_other, at_mine, at_other):
    height = rows.shape[0]
    wide = rows.astype(jnp.float32)
    inv_rms = lax.rsqrt(jnp.mean(wide * wide, axis=1, keepdims=True) + 1e-06)
    scaled = (wide * gain[...]).astype(jnp.bfloat16)
    for weight, out, at in ((mine, out_mine, at_mine), (other, out_other, at_other)):
        product = jnp.dot(scaled, weight[...], preferred_element_type=jnp.float32)
        out[at : at + height, :] = (product * inv_rms).astype(jnp.bfloat16)


def early_body(count, *refs):
    rows = refs[:count]
    gain, mine, other, cache, out_mine, out_other, held, sems, out_sems = refs[count:]
    copies = [pltpu.make_async_copy(r, held.at[k], sems.at[k]) for k, r in enumerate(rows)]
    for copy in copies:
        copy.start()
    where = places(EARLY, 0)
    stores = []
    for k, copy in enumerate(copies):
        copy.wait()
        project_block(held[k], gain, mine, other, out_mine, out_other, k * POS, k * POS)
        stores.append(store_block(out_mine, k, where[k], cache, out_sems.at[k]))
    for store in stores:
        store.wait()


def project_early(rows, gain, weights):
    count = len(rows)
    height = POS * count
    shape = pltpu.VMEM((height, WIDE), jnp.bfloat16)
    return pl.pallas_call(
        functools.partial(early_body, count),
        out_shape=(jax.ShapeDtypeStruct((2 * RING * POS, WIDE), jnp.bfloat16), shape, shape),
        in_specs=[ANY] * count + [VMEM] * 3,
        out_specs=(ANY, VMEM, VMEM),
        scratch_shapes=[
            pltpu.VMEM((count, POS, 2048), jnp.bfloat16),
            pltpu.SemaphoreType.DMA((count,)),
            pltpu.SemaphoreType.DMA((count,)),
        ],
        compiler_params=LIMIT,
        cost_estimate=pl.CostEstimate(
            flops=height * 2048 * 512, bytes_accessed=height * 2048 * 2, transcendentals=0
        ),
    )(*rows, gain, *weights)


def late_body(rows, gain, mine, other, before, out_mine, out_other):
    held = before.shape[0]
    out_other[:held, :] = before[...]
    project_block(rows[...], gain, mine, other, out_mine, out_other, 0, held)


def project_late(rows, gain, weights, before):
    return pl.pallas_call(
        late_body,
        out_shape=(
            pltpu.VMEM((POS, WIDE), jnp.bfloat16),
            pltpu.VMEM((before.shape[0] + POS, WIDE), jnp.bfloat16),
        ),
        in_specs=[VMEM] * 5,
        out_specs=(VMEM, VMEM),
        compiler_params=LIMIT,
    )(rows, gain, *weights, before)


def places(kinds, partner):
    at, core = lax.axis_index("y"), lax.axis_index("c")
    sign = (1 - 2 * core) * (2 * partner - 1)
    return [
        (at + sign * hops + RING) % RING * 2 + (core + partner + crossed) % 2
        for hops, crossed in kinds
    ]


def store_block(ref, row, place, cache, sem):
    block = ref.at[row * POS : (row + 1) * POS, :]
    start = pl.multiple_of(place * POS, POS)
    copy = pltpu.make_async_copy(block, cache.at[pl.ds(start, POS), :], sem)
    copy.start()
    return copy


def read_parts(small):
    lane = lax.broadcasted_iota(jnp.int32, (2, WIDE), 1)
    head = lax.broadcasted_iota(jnp.int32, (2, WIDE), 0)
    both = jnp.broadcast_to(small[0:1, :], (2, WIDE))
    new = jnp.broadcast_to(small[1:2, :], (2, WIDE))
    fresh = jnp.sum(jnp.where(lane == head, small[2:3, :], 0.0), axis=1, keepdims=True)
    keyed = jnp.where(lane < HEAD, jnp.where(head == 0, both, pltpu.roll(both, HEAD, 1)), 0.0)
    own = jnp.sum(keyed * new, axis=1, keepdims=True) * FACTOR
    return keyed.astype(jnp.bfloat16), new, own, fresh


def finish_body(gates, small, early, late, swapped, cache_in, cache, gate_out, read, sems):
    del cache_in
    heres, here, there = places(EARLY, 0), places(LATE, 0), places(EARLY + LATE, 1)
    copies = []
    for ref, where in ((late, here), (swapped, there)):
        for row, place in enumerate(where):
            copies.append(store_block(ref, row, place, cache, sems.at[len(copies)]))
    gate_out[...] = jnp.concatenate([gates[p] for p in range(2 * RING)], axis=1)
    query, new, own, fresh = read_parts(small)
    top, scores = own, []
    for ref, where in ((early, heres), (late, here), (swapped, there)):
        raw = lax.dot_general(
            query, ref[...], (((1,), (1,)), ((), ())), preferred_element_type=jnp.float32
        )
        gate = jnp.concatenate([gates[place] for place in where], axis=1)
        scores.append(raw * FACTOR + fresh - gate)
        top = jnp.maximum(top, jnp.max(scores[-1], axis=1, keepdims=True))
    total = jnp.exp(own - top)
    numer = total * new
    for ref, score in zip((early, late, swapped), scores):
        expo = jnp.exp(score - top)
        total += jnp.sum(expo, axis=1, keepdims=True)
        numer += jnp.dot(
            expo.astype(jnp.bfloat16), ref[...], preferred_element_type=jnp.float32
        )
    result = numer / total
    lane = lax.broadcasted_iota(jnp.int32, (1, WIDE), 1)
    shifted = pltpu.roll(result, HEAD, 1)
    read[...] = jnp.where(lane < HEAD, shifted[:1], result[1:]).astype(jnp.bfloat16)
    for copy in copies:
        copy.wait()


def finish(gates, small, early, late, swapped, cache):
    return pl.pallas_call(
        finish_body,
        out_shape=(
            jax.ShapeDtypeStruct((2 * RING * POS, WIDE), jnp.bfloat16),
            jax.ShapeDtypeStruct((2, 2 * RING * POS), jnp.float32),
            jax.ShapeDtypeStruct((1, WIDE), jnp.bfloat16),
        ),
        in_specs=[VMEM] * 5 + [ANY],
        out_specs=(ANY, VMEM, VMEM),
        scratch_shapes=[pltpu.SemaphoreType.DMA((len(EARLY) + 2 * len(LATE),))],
        input_output_aliases={5: 0},
        compiler_params=LIMIT,
    )(on_chip(gates), on_chip(small), on_chip(early), on_chip(late), on_chip(swapped), cache)


def per_device(tokens, norm_gain, key_weight, value_weight, cum_gate, new_gate, new_query, new_kv):
    block = tokens[0]
    tp = ("y", "c")
    ahead = [lax.ppermute(block, tp, AHEAD)]

    local = jnp.concatenate([key_weight, value_weight], axis=1)
    spread = jnp.broadcast_to(local[None], (32,) + local.shape)
    gain = jnp.broadcast_to(norm_gain[None], (1, 2048))
    small = jnp.concatenate(
        [
            new_query.astype(jnp.float32),
            new_kv[0].astype(jnp.float32),
            jnp.pad(new_gate, ((0, 0), (0, WIDE - 2))),
        ],
        axis=0,
    )
    gate_parts = cum_gate[0].reshape(2 * RING, 2, POS)
    fellow = lax.ppermute(block, "c", SWAP)
    fellow, gain, small, gate_parts, spread = lax.optimization_barrier(
        (fellow, gain, small, gate_parts, spread)
    )
    crossed = [lax.ppermute(fellow, tp, AHEAD)]
    gathered = lax.all_to_all(spread, ("z", "x"), 0, 0, tiled=True)
    mine = gathered.reshape(2048, WIDE)
    weights = [on_chip(mine), on_chip(lax.ppermute(mine, "c", SWAP))]

    for step in (2, 3, 4):
        ahead.append(lax.ppermute(ahead[-1], tp, AHEAD))
        if step < 4:
            crossed.append(lax.ppermute(crossed[-1], tp, AHEAD))
    gates = lax.all_to_all(gate_parts, tp, split_axis=0, concat_axis=0, tiled=True)

    gain = on_chip(gain)
    first = [block]
    for pair in zip(ahead, crossed):
        first += pair
    cache, early, other = project_early(first, gain, weights)
    late, others = project_late(on_chip(ahead[3]), gain, weights, on_chip(other))
    swapped = lax.ppermute(others, "c", SWAP)
    cache, gate_out, read = finish(gates, small, early, late, swapped, cache)
    return (cache[None, None], gate_out[None], read)


def solution(mesh):
    fine = Mesh(mesh.devices.reshape(8, 4, 8, 2), ("z", "x", "y", "c"))
    sp, tp = ("z", "x"), ("y", "c")
    in_specs = (
        P(sp, tp, None),
        P(),
        P(sp, tp),
        P(sp, tp),
        P(sp, None, tp),
        P(sp, tp),
        P(sp, tp),
        P(sp, tp, None),
    )
    out_specs = (P(sp, tp, None, None), P(sp, tp, None), P(sp, tp))
    return jax.shard_map(
        per_device, mesh=fine, in_specs=in_specs, out_specs=out_specs, check_vma=False
    )
```

time: 96.5 us -> 96 us (level)
  waiting for transfers between devices: 25 us -> 27.4 us
  Pallas kernels: 10.8 us -> 8.92 us
    ppermute x1, waiting for transfers between devices: 0.01 us -> 5.59 us  [per_device(): crossed = [lax.ppermute(fellow, tp, AHEAD)]]
    ppermute x2, waiting for transfers between devices: 6.93 us -> 2.19 us  [per_device(): crossed.append(lax.ppermute(crossed[-1], tp, AHEAD))]
    pallas_call x3 -> x2, Pallas kernels: 8.04 us -> 6.86 us  [the longest x1 5.09 us: project_early(): pl.pallas_call(functools.partial(early_body, count), out_shape=(jax.Shape...]
  transfers between devices with their start and end apart: 11 -> 11, of which waited for: 6 -> 8; matrix products, arithmetic and copies ran while one was open for 2% -> 2% of each run, Pallas kernels for 7% -> 5%
where the time goes in v1:
time: 96 us; the launch traced here: 95.3 us
  starting transfers between devices  41.6 us (43%)
  waiting for transfers between devices  27.4 us (29%)
  blocking collectives  14.1 us (15%)
  Pallas kernels  8.92 us (9%)
  local copies, waits for them, and re-layouts  2.38 us (2%)
    all_to_all x1, blocking collectives, per_device(): lax.all_to_all(gate_parts, tp, split_axis=0, concat_axis=0, tiled=True)  14.1 us
    all_to_all x1, starting transfers between devices, per_device(): gathered = lax.all_to_all(spread, ('z', 'x'), 0, 0, tiled=True)  10.7 us
    ppermute x3, waiting for transfers between devices, per_device(): ahead.append(lax.ppermute(ahead[-1], tp, AHEAD))  10.5 us
    ppermute x1, starting transfers between devices, per_device(): fellow = lax.ppermute(block, 'c', SWAP)  8.75 us
    ppermute x3, starting transfers between devices, per_device(): ahead.append(lax.ppermute(ahead[-1], tp, AHEAD))  8.04 us
    ppermute x1, waiting for transfers between devices, per_device(): ahead = [lax.ppermute(block, tp, AHEAD)]  6.69 us
    ppermute x2, starting transfers between devices, per_device(): crossed.append(lax.ppermute(crossed[-1], tp, AHEAD))  5.65 us
    ppermute x1, waiting for transfers between devices, per_device(): crossed = [lax.ppermute(fellow, tp, AHEAD)]  5.59 us
  transfers between devices with their start and end apart: 11, of which 8 were waited for; matrix products, arithmetic and copies ran while one was open for 2% of the time, Pallas kernels for 5%

profile of v1, /device:TPU:1, one launch (start us, length us, event | category | flops | bytes accessed | tf_op | source)
XLA Modules:
  0.0 95.3 jit_solution(5762239925954622897)
XLA Ops:
  0.6 0.0 copy-start.5
  0.6 8.7 %collective-permute-start = (bf16[192,2048]{1,0:T(8,128)(2,1)}, bf16[192,2048]{1,0:T(8,128)(2,1)S(1)}, u32[]{:S(2)}, u32[]{:S(2)}) collective-permute-start(bf16[192,2048]{1,0:T(8,128)(2,1)} %bitcast.11), channel_id=1, source_target_pairs={{0,1},{1,0},{2,3},{3,2},{4,5},{5,4},{6,7},{7,6},{8,9},{9,8},{10,11... | collective-permute-start | bytes 2359304 | tf_op jit(solution)/shard_map/ppermute | solution.py:189
  9.4 1.9 %collective-permute-start.1 = (bf16[192,2048]{1,0:T(8,128)(2,1)}, bf16[192,2048]{1,0:T(8,128)(2,1)S(1)}, u32[]{:S(2)}, u32[]{:S(2)}) collective-permute-start(bf16[192,2048]{1,0:T(8,128)(2,1)} %bitcast.12), channel_id=1, source_target_pairs={{0,2},{1,15},{2,4},{3,1},{4,6},{5,3},{6,8},{7,5},{8,10},{9,7},{10,... | collective-permute-start | bytes 2359304 | tf_op jit(solution)/shard_map/ppermute | solution.py:175
  11.3 0.0 copy-done.5
  11.3 0.0 copy-start.6
  11.4 0.0 copy-start.2
  11.4 0.0 copy-start.3
  11.4 0.8 reshape_squeeze.3
  12.2 0.0 copy-done.6
  12.2 0.0 copy-start.4
  12.2 0.6 copy-done.4
  12.9 0.0 copy-done.2
  12.9 0.0 copy-done.3
  12.9 0.1 pad_maximum_fusion
  13.0 0.0 collective-permute-done
  13.0 0.0 copy-start
  13.0 0.9 broadcast_in_dim.16
  13.9 0.0 copy-start.1
  13.9 2.0 %collective-permute-start.2 = (bf16[192,2048]{1,0:T(8,128)(2,1)S(1)}, bf16[192,2048]{1,0:T(8,128)(2,1)S(1)}, u32[]{:S(2)}, u32[]{:S(2)}) collective-permute-start(bf16[192,2048]{1,0:T(8,128)(2,1)S(1)} %collective-permute-done), channel_id=1, source_target_pairs={{0,2},{1,15},{2,4},{3,1},{4,6},{5,3},{6,8},{7,5},{8,10},{9,7},{10,... | collective-permute-start | bytes 2359304 | tf_op jit(solution)/shard_map/ppermute | solution.py:193
  15.9 6.7 %collective-permute-done.1.refs_1_ = bf16[192,2048]{1,0:T(8,128)(2,1)S(1)} collective-permute-done((bf16[192,2048]{1,0:T(8,128)(2,1)}, bf16[192,2048]{1,0:T(8,128)(2,1)S(1)}, u32[]{:S(2)}, u32[]{:S(2)}) %collective-permute-start.1) | collective-permute-done | bytes 786464 | tf_op jit(solution)/shard_map/ppermute | solution.py:175
  22.6 2.8 %collective-permute-start.3 = (bf16[192,2048]{1,0:T(8,128)(2,1)S(1)}, bf16[192,2048]{1,0:T(8,128)(2,1)}, u32[]{:S(2)}, u32[]{:S(2)}) collective-permute-start(bf16[192,2048]{1,0:T(8,128)(2,1)S(1)} %collective-permute-done.1.refs_1_), channel_id=1, source_target_pairs={{0,2},{1,15},{2,4},{3,1},{4,6},{5,3},{6,8},{7,5},{8,10},{9,7},{10,... | collective-permute-start | bytes 2359304 | tf_op jit(solution)/shard_map/ppermute | solution.py:199
  25.5 5.6 %collective-permute-done.2.refs_2_ = bf16[192,2048]{1,0:T(8,128)(2,1)S(1)} collective-permute-done((bf16[192,2048]{1,0:T(8,128)(2,1)S(1)}, bf16[192,2048]{1,0:T(8,128)(2,1)S(1)}, u32[]{:S(2)}, u32[]{:S(2)}) %collective-permute-start.2) | collective-permute-done | bytes 786464 | tf_op jit(solution)/shard_map/ppermute | solution.py:193
  31.1 2.8 %collective-permute-start.4 = (bf16[192,2048]{1,0:T(8,128)(2,1)S(1)}, bf16[192,2048]{1,0:T(8,128)(2,1)}, u32[]{:S(2)}, u32[]{:S(2)}) collective-permute-start(bf16[192,2048]{1,0:T(8,128)(2,1)S(1)} %collective-permute-done.2.refs_2_), channel_id=1, source_target_pairs={{0,2},{1,15},{2,4},{3,1},{4,6},{5,3},{6,8},{7,5},{8,10},{9,7},{10,... | collective-permute-start | bytes 2359304 | tf_op jit(solution)/shard_map/ppermute | solution.py:201
  33.9 10.7 %all-to-all-start.1 = ((bf16[32,64,128]{2,1,0:T(8,128)(2,1)}), bf16[32,64,128]{2,1,0:T(8,128)(2,1)S(1)}, u32[]{:S(2)}, u32[]{:S(2)}) async-start(bf16[32,64,128]{2,1,0:T(8,128)(2,1)} %broadcast_in_dim.16), calls=%async_computation.1 | async-start | bytes 1048576 | tf_op jit(solution)/shard_map/all_to_all | solution.py:194
  44.6 0.0 collective-permute-done.3.refs_3_
  44.7 2.1 %collective-permute-start.5 = (bf16[192,2048]{1,0:T(8,128)(2,1)}, bf16[192,2048]{1,0:T(8,128)(2,1)}, u32[]{:S(2)}, u32[]{:S(2)}) collective-permute-start(bf16[192,2048]{1,0:T(8,128)(2,1)} %collective-permute-done.3.refs_3_), channel_id=1, source_target_pairs={{0,2},{1,15},{2,4},{3,1},{4,6},{5,3},{6,8},{7,5},{8,10},{9,7},{10,... | collective-permute-start | bytes 2359304 | tf_op jit(solution)/shard_map/ppermute | solution.py:199
  46.7 1.3 %collective-permute-done.4.refs_4_ = bf16[192,2048]{1,0:T(8,128)(2,1)} collective-permute-done((bf16[192,2048]{1,0:T(8,128)(2,1)S(1)}, bf16[192,2048]{1,0:T(8,128)(2,1)}, u32[]{:S(2)}, u32[]{:S(2)}) %collective-permute-start.4) | collective-permute-done | bytes 786464 | tf_op jit(solution)/shard_map/ppermute | solution.py:201
  48.0 2.8 %collective-permute-start.6 = (bf16[192,2048]{1,0:T(8,128)(2,1)}, bf16[192,2048]{1,0:T(8,128)(2,1)}, u32[]{:S(2)}, u32[]{:S(2)}) collective-permute-start(bf16[192,2048]{1,0:T(8,128)(2,1)} %collective-permute-done.4.refs_4_), channel_id=1, source_target_pairs={{0,2},{1,15},{2,4},{3,1},{4,6},{5,3},{6,8},{7,5},{8,10},{9,7},{10,... | collective-permute-start | bytes 2359304 | tf_op jit(solution)/shard_map/ppermute | solution.py:201
  50.9 7.1 %collective-permute-done.5.refs_5_ = bf16[192,2048]{1,0:T(8,128)(2,1)} collective-permute-done((bf16[192,2048]{1,0:T(8,128)(2,1)}, bf16[192,2048]{1,0:T(8,128)(2,1)}, u32[]{:S(2)}, u32[]{:S(2)}) %collective-permute-start.5) | collective-permute-done | bytes 786464 | tf_op jit(solution)/shard_map/ppermute | solution.py:199
  58.0 3.2 %collective-permute-start.8 = (bf16[192,2048]{1,0:T(8,128)(2,1)}, bf16[192,2048]{1,0:T(8,128)(2,1)}, u32[]{:S(2)}, u32[]{:S(2)}) collective-permute-start(bf16[192,2048]{1,0:T(8,128)(2,1)} %collective-permute-done.5.refs_5_), channel_id=1, source_target_pairs={{0,2},{1,15},{2,4},{3,1},{4,6},{5,3},{6,8},{7,5},{8,10},{9,7},{10,... | collective-permute-start | bytes 2359304 | tf_op jit(solution)/shard_map/ppermute | solution.py:199
  61.2 0.6 all-to-all-done.1
  61.7 1.9 %collective-permute-start.7 = (bf16[2048,128]{1,0:T(8,128)(2,1)S(1)}, bf16[2048,128]{1,0:T(8,128)(2,1)S(1)}, u32[]{:S(2)}, u32[]{:S(2)}) collective-permute-start(bf16[2048,128]{1,0:T(8,128)(2,1)S(1)} %bitcast.8), channel_id=1, source_target_pairs={{0,1},{1,0},{2,3},{3,2},{4,5},{5,4},{6,7},{7,6},{8,9},{9,8},{10,11... | collective-permute-start | bytes 1572872 | tf_op jit(solution)/shard_map/ppermute | solution.py:196
  63.7 1.9 %collective-permute-done.7.refs_9_.other = bf16[2048,128]{1,0:T(8,128)(2,1)S(1)} collective-permute-done((bf16[2048,128]{1,0:T(8,128)(2,1)S(1)}, bf16[2048,128]{1,0:T(8,128)(2,1)S(1)}, u32[]{:S(2)}, u32[]{:S(2)}) %collective-permute-start.7) | collective-permute-done | bytes 524320 | tf_op jit(solution)/shard_map/ppermute | solution.py:196
  65.5 0.9 collective-permute-done.6.refs_6_
  66.4 0.0 copy-done
  66.4 0.0 copy-done.1
  66.4 5.1 %shard_map.103 = (bf16[3072,128]{1,0:T(8,128)(2,1)}, bf16[1344,128]{1,0:T(8,128)(2,1)S(1)}, bf16[1344,128]{1,0:T(8,128)(2,1)S(1)}) custom-call(bf16[192,2048]{1,0:T(8,128)(2,1)S(1)} %bitcast.13, bf16[192,2048]{1,0:T(8,128)(2,1)S(1)} %collective-permute-done.1.refs_1_, bf16[192,2048]{1,0:T(8,128)(2,1)S(1)} %collective-permute-done.2.refs_2_, ...), custom_call_target="tpu_custom_call" | custom-call | flops 1409286144 | bytes 5505024 | tf_op jit(solution)/shard_map/pallas_call | solution.py:59
  71.5 3.3 %collective-permute-done.8.rows = bf16[192,2048]{1,0:T(8,128)(2,1)} collective-permute-done((bf16[192,2048]{1,0:T(8,128)(2,1)}, bf16[192,2048]{1,0:T(8,128)(2,1)}, u32[]{:S(2)}, u32[]{:S(2)}) %collective-permute-start.8) | collective-permute-done | bytes 786464 | tf_op jit(solution)/shard_map/ppermute | solution.py:199
  74.9 1.8 %shard_map.104 = (bf16[192,128]{1,0:T(8,128)(2,1)S(1)}, bf16[1536,128]{1,0:T(8,128)(2,1)S(1)}) custom-call(bf16[192,2048]{1,0:T(8,128)(2,1)} %collective-permute-done.8.rows, f32[1,2048]{1,0:T(1,128)S(1)} %bitcast.15, bf16[2048,128]{1,0:T(8,128)(2,1)S(1)} %bitcast.10, bf16[2048,128]{1,0:T(8,128)(2,1)S(1)} %collective-permute-done.7.refs_9_.other, ...), custom_call_target="tpu_custom_call" | custom-call | tf_op jit(solution)/shard_map/pallas_call | solution.py:83
  76.6 2.6 %collective-permute-start.9 = (bf16[1536,128]{1,0:T(8,128)(2,1)S(1)}, bf16[1536,128]{1,0:T(8,128)(2,1)S(1)}, u32[]{:S(2)}, u32[]{:S(2)}) collective-permute-start(bf16[1536,128]{1,0:T(8,128)(2,1)S(1)} %get-tuple-element.24), channel_id=1, source_target_pairs={{0,1},{1,0},{2,3},{3,2},{4,5},{5,4},{6,7},{7,6},{8,9},{9,8},{10,11... | collective-permute-start | bytes 1179656 | tf_op jit(solution)/shard_map/ppermute | solution.py:210
  79.2 14.1 %all_to_all.10.gates = f32[16,2,192]{2,1,0:T(2,128)S(1)} all-to-all(f32[16,2,192]{2,1,0:T(2,128)S(1)} %reshape_squeeze.3), channel_id=1, replica_groups=mesh['z'=8,'x'=4,'y'=8,'c'=2] {'y','c'}, dimensions={0} | all-to-all | bytes 49152 | tf_op jit(solution)/shard_map/all_to_all | solution.py:202
  93.3 0.0 collective-permute-done.9.swapped
  93.3 2.1 %shard_map.105 = (bf16[3072,128]{1,0:T(8,128)(2,1)}, f32[2,3072]{1,0:T(2,128)}, bf16[1,128]{1,0:T(2,128)(2,1)}) custom-call(f32[16,2,192]{2,1,0:T(2,128)S(1)} %all_to_all.10.gates, f32[3,128]{1,0:T(4,128)S(1)} %select_maximum_fusion.small, bf16[1344,128]{1,0:T(8,128)(2,1)S(1)} %get-tuple-element.21.early, ...), custom_call_target="tpu_custom_call", output_to_operand_aliasing={{0}: (5, {})} | custom-call | tf_op jit(solution)/shard_map/pallas_call | solution.py:157
  (3 shorter events, 0.0 us)
Async XLA Ops:
  0.6 10.7 %copy-start.5 = (bf16[1,128]{1,0:T(2,128)(2,1)S(1)}, bf16[1,128]{1,0:T(2,128)(2,1)}, u32[]{:S(2)}) copy-start(bf16[1,128]{1,0:T(2,128)(2,1)} %param.14) | copy-start | bytes 772
  0.6 12.3 %collective-permute-start = (bf16[192,2048]{1,0:T(8,128)(2,1)}, bf16[192,2048]{1,0:T(8,128)(2,1)S(1)}, u32[]{:S(2)}, u32[]{:S(2)}) collective-permute-start(bf16[192,2048]{1,0:T(8,128)(2,1)} %bitcast.11), channel_id=1, source_target_pairs={{0,1},{1,0},{2,3},{3,2},{4,5},{5,4},{6,7},{7,6},{8,9},{9,8},{10,11... | collective-permute-start | bytes 2359304 | tf_op jit(solution)/shard_map/ppermute | solution.py:189
  9.4 13.2 %collective-permute-start.1 = (bf16[192,2048]{1,0:T(8,128)(2,1)}, bf16[192,2048]{1,0:T(8,128)(2,1)S(1)}, u32[]{:S(2)}, u32[]{:S(2)}) collective-permute-start(bf16[192,2048]{1,0:T(8,128)(2,1)} %bitcast.12), channel_id=1, source_target_pairs={{0,2},{1,15},{2,4},{3,1},{4,6},{5,3},{6,8},{7,5},{8,10},{9,7},{10,... | collective-permute-start | bytes 2359304 | tf_op jit(solution)/shard_map/ppermute | solution.py:175
  11.3 0.8 copy-start.6
  11.4 1.5 %copy-start.2 = (bf16[64,64]{1,0:T(8,128)(2,1)S(1)}, bf16[64,64]{1,0:T(8,128)(2,1)}, u32[]{:S(2)}) copy-start(bf16[64,64]{1,0:T(8,128)(2,1)} %param.11) | copy-start | bytes 24580
  11.4 1.5 %copy-start.3 = (bf16[64,64]{1,0:T(8,128)(2,1)S(1)}, bf16[64,64]{1,0:T(8,128)(2,1)}, u32[]{:S(2)}) copy-start(bf16[64,64]{1,0:T(8,128)(2,1)} %param.10) | copy-start | bytes 24580
  12.2 0.7 copy-start.4
  13.0 53.5 %copy-start = (bf16[1,192,2048]{2,1,0:T(8,128)(2,1)S(1)}, bf16[1,192,2048]{2,1,0:T(8,128)(2,1)}, u32[]{:S(2)}) copy-start(bf16[1,192,2048]{2,1,0:T(8,128)(2,1)} %param.8) | copy-start | bytes 2359300
  13.9 52.5 %copy-start.1 = (f32[2048]{0:T(1024)S(1)}, f32[2048]{0:T(1024)}, u32[]{:S(2)}) copy-start(f32[2048]{0:T(1024)} %param.9) | copy-start | bytes 24580
  13.9 17.2 %collective-permute-start.2 = (bf16[192,2048]{1,0:T(8,128)(2,1)S(1)}, bf16[192,2048]{1,0:T(8,128)(2,1)S(1)}, u32[]{:S(2)}, u32[]{:S(2)}) collective-permute-start(bf16[192,2048]{1,0:T(8,128)(2,1)S(1)} %collective-permute-done), channel_id=1, source_target_pairs={{0,2},{1,15},{2,4},{3,1},{4,6},{5,3},{6,8},{7,5},{8,10},{9,7},{10,... | collective-permute-start | bytes 2359304 | tf_op jit(solution)/shard_map/ppermute | solution.py:193
  22.6 22.0 %collective-permute-start.3 = (bf16[192,2048]{1,0:T(8,128)(2,1)S(1)}, bf16[192,2048]{1,0:T(8,128)(2,1)}, u32[]{:S(2)}, u32[]{:S(2)}) collective-permute-start(bf16[192,2048]{1,0:T(8,128)(2,1)S(1)} %collective-permute-done.1.refs_1_), channel_id=1, source_target_pairs={{0,2},{1,15},{2,4},{3,1},{4,6},{5,3},{6,8},{7,5},{8,10},{9,7},{10,... | collective-permute-start | bytes 2359304 | tf_op jit(solution)/shard_map/ppermute | solution.py:199
  31.1 17.0 %collective-permute-start.4 = (bf16[192,2048]{1,0:T(8,128)(2,1)S(1)}, bf16[192,2048]{1,0:T(8,128)(2,1)}, u32[]{:S(2)}, u32[]{:S(2)}) collective-permute-start(bf16[192,2048]{1,0:T(8,128)(2,1)S(1)} %collective-permute-done.2.refs_2_), channel_id=1, source_target_pairs={{0,2},{1,15},{2,4},{3,1},{4,6},{5,3},{6,8},{7,5},{8,10},{9,7},{10,... | collective-permute-start | bytes 2359304 | tf_op jit(solution)/shard_map/ppermute | solution.py:201
  33.9 27.8 %all-to-all-start.1 = ((bf16[32,64,128]{2,1,0:T(8,128)(2,1)}), bf16[32,64,128]{2,1,0:T(8,128)(2,1)S(1)}, u32[]{:S(2)}, u32[]{:S(2)}) async-start(bf16[32,64,128]{2,1,0:T(8,128)(2,1)} %broadcast_in_dim.16), calls=%async_computation.1 | async-start | bytes 1048576 | tf_op jit(solution)/shard_map/all_to_all | solution.py:194
  44.7 13.3 %collective-permute-start.5 = (bf16[192,2048]{1,0:T(8,128)(2,1)}, bf16[192,2048]{1,0:T(8,128)(2,1)}, u32[]{:S(2)}, u32[]{:S(2)}) collective-permute-start(bf16[192,2048]{1,0:T(8,128)(2,1)} %collective-permute-done.3.refs_3_), channel_id=1, source_target_pairs={{0,2},{1,15},{2,4},{3,1},{4,6},{5,3},{6,8},{7,5},{8,10},{9,7},{10,... | collective-permute-start | bytes 2359304 | tf_op jit(solution)/shard_map/ppermute | solution.py:199
  48.0 18.4 %collective-permute-start.6 = (bf16[192,2048]{1,0:T(8,128)(2,1)}, bf16[192,2048]{1,0:T(8,128)(2,1)}, u32[]{:S(2)}, u32[]{:S(2)}) collective-permute-start(bf16[192,2048]{1,0:T(8,128)(2,1)} %collective-permute-done.4.refs_4_), channel_id=1, source_target_pairs={{0,2},{1,15},{2,4},{3,1},{4,6},{5,3},{6,8},{7,5},{8,10},{9,7},{10,... | collective-permute-start | bytes 2359304 | tf_op jit(solution)/shard_map/ppermute | solution.py:201
  58.0 16.9 %collective-permute-start.8 = (bf16[192,2048]{1,0:T(8,128)(2,1)}, bf16[192,2048]{1,0:T(8,128)(2,1)}, u32[]{:S(2)}, u32[]{:S(2)}) collective-permute-start(bf16[192,2048]{1,0:T(8,128)(2,1)} %collective-permute-done.5.refs_5_), channel_id=1, source_target_pairs={{0,2},{1,15},{2,4},{3,1},{4,6},{5,3},{6,8},{7,5},{8,10},{9,7},{10,... | collective-permute-start | bytes 2359304 | tf_op jit(solution)/shard_map/ppermute | solution.py:199
  61.7 3.8 %collective-permute-start.7 = (bf16[2048,128]{1,0:T(8,128)(2,1)S(1)}, bf16[2048,128]{1,0:T(8,128)(2,1)S(1)}, u32[]{:S(2)}, u32[]{:S(2)}) collective-permute-start(bf16[2048,128]{1,0:T(8,128)(2,1)S(1)} %bitcast.8), channel_id=1, source_target_pairs={{0,1},{1,0},{2,3},{3,2},{4,5},{5,4},{6,7},{7,6},{8,9},{9,8},{10,11... | collective-permute-start | bytes 1572872 | tf_op jit(solution)/shard_map/ppermute | solution.py:196
  76.6 16.7 %collective-permute-start.9 = (bf16[1536,128]{1,0:T(8,128)(2,1)S(1)}, bf16[1536,128]{1,0:T(8,128)(2,1)S(1)}, u32[]{:S(2)}, u32[]{:S(2)}) collective-permute-start(bf16[1536,128]{1,0:T(8,128)(2,1)S(1)} %get-tuple-element.24), channel_id=1, source_target_pairs={{0,1},{1,0},{2,3},{3,2},{4,5},{5,4},{6,7},{7,6},{8,9},{9,8},{10,11... | collective-permute-start | bytes 1179656 | tf_op jit(solution)/shard_map/ppermute | solution.py:210

commit v2 on v1

--- a/solution.py
+++ b/solution.py
@@ -73,23 +73,19 @@
     )(*rows, gain, *weights)
 
 
-def late_body(rows, gain, mine, other, before, out_mine, out_other):
-    held = before.shape[0]
-    out_other[:held, :] = before[...]
-    project_block(rows[...], gain, mine, other, out_mine, out_other, 0, held)
-
-
-def project_late(rows, gain, weights, before):
+def late_body(rows, gain, mine, other, out_mine, out_other):
+    project_block(rows[...], gain, mine, other, out_mine, out_other, 0, 0)
+
+
+def project_late(rows, gain, weights):
+    shape = pltpu.VMEM((POS, WIDE), jnp.bfloat16)
     return pl.pallas_call(
         late_body,
-        out_shape=(
-            pltpu.VMEM((POS, WIDE), jnp.bfloat16),
-            pltpu.VMEM((before.shape[0] + POS, WIDE), jnp.bfloat16),
-        ),
-        in_specs=[VMEM] * 5,
+        out_shape=(shape, shape),
+        in_specs=[VMEM] * 4,
         out_specs=(VMEM, VMEM),
         compiler_params=LIMIT,
-    )(rows, gain, *weights, before)
+    )(rows, gain, *weights)
 
 
 def places(kinds, partner):
@@ -120,17 +116,18 @@
     return keyed.astype(jnp.bfloat16), new, own, fresh
 
 
-def finish_body(gates, small, early, late, swapped, cache_in, cache, gate_out, read, sems):
-    del cache_in
-    heres, here, there = places(EARLY, 0), places(LATE, 0), places(EARLY + LATE, 1)
+def finish_body(gates, small, *refs):
+    cache, gate_out, read, sems = refs[-4:]
+    kinds = ((EARLY, 0), (LATE, 0), (EARLY, 1), (LATE, 1))
+    pieces = [(ref, places(*kind)) for ref, kind in zip(refs, kinds)]
     copies = []
-    for ref, where in ((late, here), (swapped, there)):
+    for ref, where in pieces[1:]:
         for row, place in enumerate(where):
             copies.append(store_block(ref, row, place, cache, sems.at[len(copies)]))
     gate_out[...] = jnp.concatenate([gates[p] for p in range(2 * RING)], axis=1)
     query, new, own, fresh = read_parts(small)
     top, scores = own, []
-    for ref, where in ((early, heres), (late, here), (swapped, there)):
+    for ref, where in pieces:
         raw = lax.dot_general(
             query, ref[...], (((1,), (1,)), ((), ())), preferred_element_type=jnp.float32
         )
@@ -139,7 +136,7 @@
         top = jnp.maximum(top, jnp.max(scores[-1], axis=1, keepdims=True))
     total = jnp.exp(own - top)
     numer = total * new
-    for ref, score in zip((early, late, swapped), scores):
+    for (ref, _), score in zip(pieces, scores):
         expo = jnp.exp(score - top)
         total += jnp.sum(expo, axis=1, keepdims=True)
         numer += jnp.dot(
@@ -153,7 +150,7 @@
         copy.wait()
 
 
-def finish(gates, small, early, late, swapped, cache):
+def finish(gates, small, pieces, cache):
     return pl.pallas_call(
         finish_body,
         out_shape=(
@@ -161,12 +158,12 @@
             jax.ShapeDtypeStruct((2, 2 * RING * POS), jnp.float32),
             jax.ShapeDtypeStruct((1, WIDE), jnp.bfloat16),
         ),
-        in_specs=[VMEM] * 5 + [ANY],
+        in_specs=[VMEM] * 6 + [ANY],
         out_specs=(ANY, VMEM, VMEM),
         scratch_shapes=[pltpu.SemaphoreType.DMA((len(EARLY) + 2 * len(LATE),))],
-        input_output_aliases={5: 0},
+        input_output_aliases={6: 0},
         compiler_params=LIMIT,
-    )(on_chip(gates), on_chip(small), on_chip(early), on_chip(late), on_chip(swapped), cache)
+    )(on_chip(gates), on_chip(small), *[on_chip(p) for p in pieces], cache)
 
 
 def per_device(tokens, norm_gain, key_weight, value_weight, cum_gate, new_gate, new_query, new_kv):
@@ -206,9 +203,11 @@
     for pair in zip(ahead, crossed):
         first += pair
     cache, early, other = project_early(first, gain, weights)
-    late, others = project_late(on_chip(ahead[3]), gain, weights, on_chip(other))
-    swapped = lax.ppermute(others, "c", SWAP)
-    cache, gate_out, read = finish(gates, small, early, late, swapped, cache)
+    early_swapped = lax.ppermute(other, "c", SWAP)
+    late, late_other = project_late(on_chip(ahead[3]), gain, weights)
+    late_swapped = lax.ppermute(late_other, "c", SWAP)
+    pieces = (early, late, early_swapped, late_swapped)
+    cache, gate_out, read = finish(gates, small, pieces, cache)
     return (cache[None, None], gate_out[None], read)
 
 

time: 96 us -> 97.2 us (1.012)
  starting transfers between devices: 41.6 us -> 45.9 us
  blocking collectives: 14.1 us -> 12.5 us
  Pallas kernels: 8.92 us -> 7.81 us
    all_to_all x1, waiting for transfers between devices: 0.58 us -> 10.9 us  [per_device(): gathered = lax.all_to_all(spread, ('z', 'x'), 0, 0, tiled=True)]
    ppermute x3, waiting for transfers between devices: 10.5 us -> 2.51 us  [per_device(): ahead.append(lax.ppermute(ahead[-1], tp, AHEAD))]
    ppermute x1 -> x2, starting transfers between devices: 2.59 us -> 6.39 us  [the longest x1 4.47 us: per_device(): late_swapped = lax.ppermute(late_other, 'c', SWAP)]
    ppermute x1, waiting for transfers between devices: 1.88 us -> 0.01 us  [per_device(): weights = [on_chip(mine), on_chip(lax.ppermute(mine, 'c', SWAP))]]
    all_to_all x1, blocking collectives: 14.1 us -> 12.5 us  [per_device(): lax.all_to_all(gate_parts, tp, split_axis=0, concat_axis=0, tiled=True)]
    pallas_call x1, Pallas kernels: 1.77 us -> 0.61 us  [project_late(): pl.pallas_call(late_body, out_shape=(shape, shape), in_specs=[VMEM] * 4,...]
  transfers between devices with their start and end apart: 11 -> 12, of which waited for: 8 -> 5; matrix products, arithmetic and copies ran while one was open for 2% -> 2% of each run, Pallas kernels for 5% -> 6%
where the time goes in v2:
time: 97.2 us; the launch traced here: 96.6 us
  starting transfers between devices  45.9 us (47%)
  waiting for transfers between devices  27 us (28%)
  blocking collectives  12.5 us (13%)
  Pallas kernels  7.81 us (8%)
  local copies, waits for them, and re-layouts  2.38 us (2%)
    all_to_all x1, blocking collectives, per_device(): lax.all_to_all(gate_parts, tp, split_axis=0, concat_axis=0, tiled=True)  12.5 us
    all_to_all x1, waiting for transfers between devices, per_device(): gathered = lax.all_to_all(spread, ('z', 'x'), 0, 0, tiled=True)  10.9 us
    all_to_all x1, starting transfers between devices, per_device(): gathered = lax.all_to_all(spread, ('z', 'x'), 0, 0, tiled=True)  10.7 us
    ppermute x1, starting transfers between devices, per_device(): fellow = lax.ppermute(block, 'c', SWAP)  8.75 us
    ppermute x3, starting transfers between devices, per_device(): ahead.append(lax.ppermute(ahead[-1], tp, AHEAD))  8.54 us
    ppermute x1, waiting for transfers between devices, per_device(): ahead = [lax.ppermute(block, tp, AHEAD)]  6.69 us
    ppermute x2, starting transfers between devices, per_device(): crossed.append(lax.ppermute(crossed[-1], tp, AHEAD))  5.65 us
    ppermute x1, waiting for transfers between devices, per_device(): crossed = [lax.ppermute(fellow, tp, AHEAD)]  5.59 us
  transfers between devices with their start and end apart: 12, of which 5 were waited for; matrix products, arithmetic and copies ran while one was open for 2% of the time, Pallas kernels for 6%

profile of v2, /device:TPU:1, one launch (start us, length us, event | category | flops | bytes accessed | tf_op | source)
XLA Modules:
  0.0 96.6 jit_solution(10303417016665995937)
XLA Ops:
  0.6 0.0 copy-start.5
  0.6 8.7 %collective-permute-start = (bf16[192,2048]{1,0:T(8,128)(2,1)}, bf16[192,2048]{1,0:T(8,128)(2,1)S(1)}, u32[]{:S(2)}, u32[]{:S(2)}) collective-permute-start(bf16[192,2048]{1,0:T(8,128)(2,1)} %bitcast.11), channel_id=1, source_target_pairs={{0,1},{1,0},{2,3},{3,2},{4,5},{5,4},{6,7},{7,6},{8,9},{9,8},{10,11... | collective-permute-start | bytes 2359304 | tf_op jit(solution)/shard_map/ppermute | solution.py:186
  9.4 1.9 %collective-permute-start.1 = (bf16[192,2048]{1,0:T(8,128)(2,1)}, bf16[192,2048]{1,0:T(8,128)(2,1)S(1)}, u32[]{:S(2)}, u32[]{:S(2)}) collective-permute-start(bf16[192,2048]{1,0:T(8,128)(2,1)} %bitcast.12), channel_id=1, source_target_pairs={{0,2},{1,15},{2,4},{3,1},{4,6},{5,3},{6,8},{7,5},{8,10},{9,7},{10,... | collective-permute-start | bytes 2359304 | tf_op jit(solution)/shard_map/ppermute | solution.py:172
  11.3 0.0 copy-done.5
  11.3 0.0 copy-start.6
  11.4 0.0 copy-start.2
  11.4 0.0 copy-start.3
  11.4 0.8 reshape_squeeze.3
  12.2 0.0 copy-done.6
  12.2 0.0 copy-start.4
  12.2 0.6 copy-done.4
  12.9 0.0 copy-done.2
  12.9 0.0 copy-done.3
  12.9 0.1 pad_maximum_fusion
  13.0 0.0 collective-permute-done
  13.0 0.0 copy-start
  13.0 0.9 broadcast_in_dim.16
  13.9 0.0 copy-start.1
  13.9 2.0 %collective-permute-start.2 = (bf16[192,2048]{1,0:T(8,128)(2,1)S(1)}, bf16[192,2048]{1,0:T(8,128)(2,1)S(1)}, u32[]{:S(2)}, u32[]{:S(2)}) collective-permute-start(bf16[192,2048]{1,0:T(8,128)(2,1)S(1)} %collective-permute-done), channel_id=1, source_target_pairs={{0,2},{1,15},{2,4},{3,1},{4,6},{5,3},{6,8},{7,5},{8,10},{9,7},{10,... | collective-permute-start | bytes 2359304 | tf_op jit(solution)/shard_map/ppermute | solution.py:190
  15.9 6.7 %collective-permute-done.1.refs_1_ = bf16[192,2048]{1,0:T(8,128)(2,1)S(1)} collective-permute-done((bf16[192,2048]{1,0:T(8,128)(2,1)}, bf16[192,2048]{1,0:T(8,128)(2,1)S(1)}, u32[]{:S(2)}, u32[]{:S(2)}) %collective-permute-start.1) | collective-permute-done | bytes 786464 | tf_op jit(solution)/shard_map/ppermute | solution.py:172
  22.6 2.8 %collective-permute-start.3 = (bf16[192,2048]{1,0:T(8,128)(2,1)S(1)}, bf16[192,2048]{1,0:T(8,128)(2,1)}, u32[]{:S(2)}, u32[]{:S(2)}) collective-permute-start(bf16[192,2048]{1,0:T(8,128)(2,1)S(1)} %collective-permute-done.1.refs_1_), channel_id=1, source_target_pairs={{0,2},{1,15},{2,4},{3,1},{4,6},{5,3},{6,8},{7,5},{8,10},{9,7},{10,... | collective-permute-start | bytes 2359304 | tf_op jit(solution)/shard_map/ppermute | solution.py:196
  25.5 5.6 %collective-permute-done.2.refs_2_ = bf16[192,2048]{1,0:T(8,128)(2,1)S(1)} collective-permute-done((bf16[192,2048]{1,0:T(8,128)(2,1)S(1)}, bf16[192,2048]{1,0:T(8,128)(2,1)S(1)}, u32[]{:S(2)}, u32[]{:S(2)}) %collective-permute-start.2) | collective-permute-done | bytes 786464 | tf_op jit(solution)/shard_map/ppermute | solution.py:190
  31.1 2.8 %collective-permute-start.4 = (bf16[192,2048]{1,0:T(8,128)(2,1)S(1)}, bf16[192,2048]{1,0:T(8,128)(2,1)}, u32[]{:S(2)}, u32[]{:S(2)}) collective-permute-start(bf16[192,2048]{1,0:T(8,128)(2,1)S(1)} %collective-permute-done.2.refs_2_), channel_id=1, source_target_pairs={{0,2},{1,15},{2,4},{3,1},{4,6},{5,3},{6,8},{7,5},{8,10},{9,7},{10,... | collective-permute-start | bytes 2359304 | tf_op jit(solution)/shard_map/ppermute | solution.py:198
  33.9 10.7 %all-to-all-start.1 = ((bf16[32,64,128]{2,1,0:T(8,128)(2,1)}), bf16[32,64,128]{2,1,0:T(8,128)(2,1)S(1)}, u32[]{:S(2)}, u32[]{:S(2)}) async-start(bf16[32,64,128]{2,1,0:T(8,128)(2,1)} %broadcast_in_dim.16), calls=%async_computation.1 | async-start | bytes 1048576 | tf_op jit(solution)/shard_map/all_to_all | solution.py:191
  44.6 0.0 collective-permute-done.3.refs_3_
  44.7 2.1 %collective-permute-start.5 = (bf16[192,2048]{1,0:T(8,128)(2,1)}, bf16[192,2048]{1,0:T(8,128)(2,1)}, u32[]{:S(2)}, u32[]{:S(2)}) collective-permute-start(bf16[192,2048]{1,0:T(8,128)(2,1)} %collective-permute-done.3.refs_3_), channel_id=1, source_target_pairs={{0,2},{1,15},{2,4},{3,1},{4,6},{5,3},{6,8},{7,5},{8,10},{9,7},{10,... | collective-permute-start | bytes 2359304 | tf_op jit(solution)/shard_map/ppermute | solution.py:196
  46.7 1.3 %collective-permute-done.4.refs_4_ = bf16[192,2048]{1,0:T(8,128)(2,1)} collective-permute-done((bf16[192,2048]{1,0:T(8,128)(2,1)S(1)}, bf16[192,2048]{1,0:T(8,128)(2,1)}, u32[]{:S(2)}, u32[]{:S(2)}) %collective-permute-start.4) | collective-permute-done | bytes 786464 | tf_op jit(solution)/shard_map/ppermute | solution.py:198
  48.0 2.8 %collective-permute-start.6 = (bf16[192,2048]{1,0:T(8,128)(2,1)}, bf16[192,2048]{1,0:T(8,128)(2,1)}, u32[]{:S(2)}, u32[]{:S(2)}) collective-permute-start(bf16[192,2048]{1,0:T(8,128)(2,1)} %collective-permute-done.4.refs_4_), channel_id=1, source_target_pairs={{0,2},{1,15},{2,4},{3,1},{4,6},{5,3},{6,8},{7,5},{8,10},{9,7},{10,... | collective-permute-start | bytes 2359304 | tf_op jit(solution)/shard_map/ppermute | solution.py:198
  50.9 10.9 %all-to-all-done.1 = bf16[32,64,128]{2,1,0:T(8,128)(2,1)S(1)} async-done(((bf16[32,64,128]{2,1,0:T(8,128)(2,1)}), bf16[32,64,128]{2,1,0:T(8,128)(2,1)S(1)}, u32[]{:S(2)}, u32[]{:S(2)}) %all-to-all-start.1) | async-done | bytes 524320 | tf_op jit(solution)/shard_map/all_to_all | solution.py:191
  61.7 1.9 %collective-permute-start.7 = (bf16[2048,128]{1,0:T(8,128)(2,1)S(1)}, bf16[2048,128]{1,0:T(8,128)(2,1)S(1)}, u32[]{:S(2)}, u32[]{:S(2)}) collective-permute-start(bf16[2048,128]{1,0:T(8,128)(2,1)S(1)} %bitcast.8), channel_id=1, source_target_pairs={{0,1},{1,0},{2,3},{3,2},{4,5},{5,4},{6,7},{7,6},{8,9},{9,8},{10,11... | collective-permute-start | bytes 1572872 | tf_op jit(solution)/shard_map/ppermute | solution.py:193
  63.7 0.0 collective-permute-done.5.refs_5_
  63.7 3.6 %collective-permute-start.8 = (bf16[192,2048]{1,0:T(8,128)(2,1)}, bf16[192,2048]{1,0:T(8,128)(2,1)S(1)}, u32[]{:S(2)}, u32[]{:S(2)}) collective-permute-start(bf16[192,2048]{1,0:T(8,128)(2,1)} %collective-permute-done.5.refs_5_), channel_id=1, source_target_pairs={{0,2},{1,15},{2,4},{3,1},{4,6},{5,3},{6,8},{7,5},{8,10},{9,7},{10,... | collective-permute-start | bytes 2359304 | tf_op jit(solution)/shard_map/ppermute | solution.py:196
  67.3 0.0 collective-permute-done.7.refs_9_.other
  67.3 0.0 collective-permute-done.6.refs_6_
  67.3 0.0 copy-done
  67.4 0.0 copy-done.1
  67.4 5.1 %shard_map.103 = (bf16[3072,128]{1,0:T(8,128)(2,1)}, bf16[1344,128]{1,0:T(8,128)(2,1)S(1)}, bf16[1344,128]{1,0:T(8,128)(2,1)S(1)}) custom-call(bf16[192,2048]{1,0:T(8,128)(2,1)S(1)} %bitcast.13, bf16[192,2048]{1,0:T(8,128)(2,1)S(1)} %collective-permute-done.1.refs_1_, bf16[192,2048]{1,0:T(8,128)(2,1)S(1)} %collective-permute-done.2.refs_2_, ...), custom_call_target="tpu_custom_call" | custom-call | flops 1409286144 | bytes 5505024 | tf_op jit(solution)/shard_map/pallas_call | solution.py:59
  72.5 1.9 %collective-permute-start.9 = (bf16[1344,128]{1,0:T(8,128)(2,1)S(1)}, bf16[1344,128]{1,0:T(8,128)(2,1)S(1)}, u32[]{:S(2)}, u32[]{:S(2)}) collective-permute-start(bf16[1344,128]{1,0:T(8,128)(2,1)S(1)} %get-tuple-element.23), channel_id=1, source_target_pairs={{0,1},{1,0},{2,3},{3,2},{4,5},{5,4},{6,7},{7,6},{8,9},{9,8},{10,11... | collective-permute-start | bytes 1032200 | tf_op jit(solution)/shard_map/ppermute | solution.py:206
  74.4 2.5 %collective-permute-done.8.rows = bf16[192,2048]{1,0:T(8,128)(2,1)S(1)} collective-permute-done((bf16[192,2048]{1,0:T(8,128)(2,1)}, bf16[192,2048]{1,0:T(8,128)(2,1)S(1)}, u32[]{:S(2)}, u32[]{:S(2)}) %collective-permute-start.8) | collective-permute-done | bytes 786464 | tf_op jit(solution)/shard_map/ppermute | solution.py:196
  76.9 0.6 shard_map.104
  77.5 4.5 %collective-permute-start.10 = (bf16[192,128]{1,0:T(8,128)(2,1)S(1)}, bf16[192,128]{1,0:T(8,128)(2,1)S(1)}, u32[]{:S(2)}, u32[]{:S(2)}) collective-permute-start(bf16[192,128]{1,0:T(8,128)(2,1)S(1)} %get-tuple-element.24), channel_id=1, source_target_pairs={{0,1},{1,0},{2,3},{3,2},{4,5},{5,4},{6,7},{7,6},{8,9},{9,8},{10,11... | collective-permute-start | bytes 147464 | tf_op jit(solution)/shard_map/ppermute | solution.py:208
  82.0 12.5 %all_to_all.10.gates = f32[16,2,192]{2,1,0:T(2,128)S(1)} all-to-all(f32[16,2,192]{2,1,0:T(2,128)S(1)} %reshape_squeeze.3), channel_id=1, replica_groups=mesh['z'=8,'x'=4,'y'=8,'c'=2] {'y','c'}, dimensions={0} | all-to-all | bytes 49152 | tf_op jit(solution)/shard_map/all_to_all | solution.py:199
  94.5 0.0 collective-permute-done.10.refs_3_
  94.5 0.0 collective-permute-done.9.refs_2_
  94.5 2.1 %shard_map.105 = (bf16[3072,128]{1,0:T(8,128)(2,1)}, f32[2,3072]{1,0:T(2,128)}, bf16[1,128]{1,0:T(2,128)(2,1)}) custom-call(f32[16,2,192]{2,1,0:T(2,128)S(1)} %all_to_all.10.gates, f32[3,128]{1,0:T(4,128)S(1)} %select_maximum_fusion.small, bf16[1344,128]{1,0:T(8,128)(2,1)S(1)} %get-tuple-element.21.refs_0_, ...), custom_call_target="tpu_custom_call", output_to_operand_aliasing={{0}: (6, {})} | custom-call | tf_op jit(solution)/shard_map/pallas_call | solution.py:154
  (3 shorter events, 0.0 us)
Async XLA Ops:
  0.6 10.7 %copy-start.5 = (bf16[1,128]{1,0:T(2,128)(2,1)S(1)}, bf16[1,128]{1,0:T(2,128)(2,1)}, u32[]{:S(2)}) copy-start(bf16[1,128]{1,0:T(2,128)(2,1)} %param.14) | copy-start | bytes 772
  0.6 12.3 %collective-permute-start = (bf16[192,2048]{1,0:T(8,128)(2,1)}, bf16[192,2048]{1,0:T(8,128)(2,1)S(1)}, u32[]{:S(2)}, u32[]{:S(2)}) collective-permute-start(bf16[192,2048]{1,0:T(8,128)(2,1)} %bitcast.11), channel_id=1, source_target_pairs={{0,1},{1,0},{2,3},{3,2},{4,5},{5,4},{6,7},{7,6},{8,9},{9,8},{10,11... | collective-permute-start | bytes 2359304 | tf_op jit(solution)/shard_map/ppermute | solution.py:186
  9.4 13.2 %collective-permute-start.1 = (bf16[192,2048]{1,0:T(8,128)(2,1)}, bf16[192,2048]{1,0:T(8,128)(2,1)S(1)}, u32[]{:S(2)}, u32[]{:S(2)}) collective-permute-start(bf16[192,2048]{1,0:T(8,128)(2,1)} %bitcast.12), channel_id=1, source_target_pairs={{0,2},{1,15},{2,4},{3,1},{4,6},{5,3},{6,8},{7,5},{8,10},{9,7},{10,... | collective-permute-start | bytes 2359304 | tf_op jit(solution)/shard_map/ppermute | solution.py:172
  11.3 0.8 copy-start.6
  11.4 1.5 %copy-start.2 = (bf16[64,64]{1,0:T(8,128)(2,1)S(1)}, bf16[64,64]{1,0:T(8,128)(2,1)}, u32[]{:S(2)}) copy-start(bf16[64,64]{1,0:T(8,128)(2,1)} %param.11) | copy-start | bytes 24580
  11.4 1.5 %copy-start.3 = (bf16[64,64]{1,0:T(8,128)(2,1)S(1)}, bf16[64,64]{1,0:T(8,128)(2,1)}, u32[]{:S(2)}) copy-start(bf16[64,64]{1,0:T(8,128)(2,1)} %param.10) | copy-start | bytes 24580
  12.2 0.7 copy-start.4
  13.0 54.4 %copy-start = (bf16[1,192,2048]{2,1,0:T(8,128)(2,1)S(1)}, bf16[1,192,2048]{2,1,0:T(8,128)(2,1)}, u32[]{:S(2)}) copy-start(bf16[1,192,2048]{2,1,0:T(8,128)(2,1)} %param.8) | copy-start | bytes 2359300
  13.9 53.5 %copy-start.1 = (f32[2048]{0:T(1024)S(1)}, f32[2048]{0:T(1024)}, u32[]{:S(2)}) copy-start(f32[2048]{0:T(1024)} %param.9) | copy-start | bytes 24580
  13.9 17.2 %collective-permute-start.2 = (bf16[192,2048]{1,0:T(8,128)(2,1)S(1)}, bf16[192,2048]{1,0:T(8,128)(2,1)S(1)}, u32[]{:S(2)}, u32[]{:S(2)}) collective-permute-start(bf16[192,2048]{1,0:T(8,128)(2,1)S(1)} %collective-permute-done), channel_id=1, source_target_pairs={{0,2},{1,15},{2,4},{3,1},{4,6},{5,3},{6,8},{7,5},{8,10},{9,7},{10,... | collective-permute-start | bytes 2359304 | tf_op jit(solution)/shard_map/ppermute | solution.py:190
  22.6 22.0 %collective-permute-start.3 = (bf16[192,2048]{1,0:T(8,128)(2,1)S(1)}, bf16[192,2048]{1,0:T(8,128)(2,1)}, u32[]{:S(2)}, u32[]{:S(2)}) collective-permute-start(bf16[192,2048]{1,0:T(8,128)(2,1)S(1)} %collective-permute-done.1.refs_1_), channel_id=1, source_target_pairs={{0,2},{1,15},{2,4},{3,1},{4,6},{5,3},{6,8},{7,5},{8,10},{9,7},{10,... | collective-permute-start | bytes 2359304 | tf_op jit(solution)/shard_map/ppermute | solution.py:196
  31.1 17.0 %collective-permute-start.4 = (bf16[192,2048]{1,0:T(8,128)(2,1)S(1)}, bf16[192,2048]{1,0:T(8,128)(2,1)}, u32[]{:S(2)}, u32[]{:S(2)}) collective-permute-start(bf16[192,2048]{1,0:T(8,128)(2,1)S(1)} %collective-permute-done.2.refs_2_), channel_id=1, source_target_pairs={{0,2},{1,15},{2,4},{3,1},{4,6},{5,3},{6,8},{7,5},{8,10},{9,7},{10,... | collective-permute-start | bytes 2359304 | tf_op jit(solution)/shard_map/ppermute | solution.py:198
  33.9 27.8 %all-to-all-start.1 = ((bf16[32,64,128]{2,1,0:T(8,128)(2,1)}), bf16[32,64,128]{2,1,0:T(8,128)(2,1)S(1)}, u32[]{:S(2)}, u32[]{:S(2)}) async-start(bf16[32,64,128]{2,1,0:T(8,128)(2,1)} %broadcast_in_dim.16), calls=%async_computation.1 | async-start | bytes 1048576 | tf_op jit(solution)/shard_map/all_to_all | solution.py:191
  44.7 19.0 %collective-permute-start.5 = (bf16[192,2048]{1,0:T(8,128)(2,1)}, bf16[192,2048]{1,0:T(8,128)(2,1)}, u32[]{:S(2)}, u32[]{:S(2)}) collective-permute-start(bf16[192,2048]{1,0:T(8,128)(2,1)} %collective-permute-done.3.refs_3_), channel_id=1, source_target_pairs={{0,2},{1,15},{2,4},{3,1},{4,6},{5,3},{6,8},{7,5},{8,10},{9,7},{10,... | collective-permute-start | bytes 2359304 | tf_op jit(solution)/shard_map/ppermute | solution.py:196
  48.0 19.3 %collective-permute-start.6 = (bf16[192,2048]{1,0:T(8,128)(2,1)}, bf16[192,2048]{1,0:T(8,128)(2,1)}, u32[]{:S(2)}, u32[]{:S(2)}) collective-permute-start(bf16[192,2048]{1,0:T(8,128)(2,1)} %collective-permute-done.4.refs_4_), channel_id=1, source_target_pairs={{0,2},{1,15},{2,4},{3,1},{4,6},{5,3},{6,8},{7,5},{8,10},{9,7},{10,... | collective-permute-start | bytes 2359304 | tf_op jit(solution)/shard_map/ppermute | solution.py:198
  61.7 5.6 %collective-permute-start.7 = (bf16[2048,128]{1,0:T(8,128)(2,1)S(1)}, bf16[2048,128]{1,0:T(8,128)(2,1)S(1)}, u32[]{:S(2)}, u32[]{:S(2)}) collective-permute-start(bf16[2048,128]{1,0:T(8,128)(2,1)S(1)} %bitcast.8), channel_id=1, source_target_pairs={{0,1},{1,0},{2,3},{3,2},{4,5},{5,4},{6,7},{7,6},{8,9},{9,8},{10,11... | collective-permute-start | bytes 1572872 | tf_op jit(solution)/shard_map/ppermute | solution.py:193
  63.7 13.2 %collective-permute-start.8 = (bf16[192,2048]{1,0:T(8,128)(2,1)}, bf16[192,2048]{1,0:T(8,128)(2,1)S(1)}, u32[]{:S(2)}, u32[]{:S(2)}) collective-permute-start(bf16[192,2048]{1,0:T(8,128)(2,1)} %collective-permute-done.5.refs_5_), channel_id=1, source_target_pairs={{0,2},{1,15},{2,4},{3,1},{4,6},{5,3},{6,8},{7,5},{8,10},{9,7},{10,... | collective-permute-start | bytes 2359304 | tf_op jit(solution)/shard_map/ppermute | solution.py:196
  72.5 22.0 %collective-permute-start.9 = (bf16[1344,128]{1,0:T(8,128)(2,1)S(1)}, bf16[1344,128]{1,0:T(8,128)(2,1)S(1)}, u32[]{:S(2)}, u32[]{:S(2)}) collective-permute-start(bf16[1344,128]{1,0:T(8,128)(2,1)S(1)} %get-tuple-element.23), channel_id=1, source_target_pairs={{0,1},{1,0},{2,3},{3,2},{4,5},{5,4},{6,7},{7,6},{8,9},{9,8},{10,11... | collective-permute-start | bytes 1032200 | tf_op jit(solution)/shard_map/ppermute | solution.py:206
  77.5 17.0 %collective-permute-start.10 = (bf16[192,128]{1,0:T(8,128)(2,1)S(1)}, bf16[192,128]{1,0:T(8,128)(2,1)S(1)}, u32[]{:S(2)}, u32[]{:S(2)}) collective-permute-start(bf16[192,128]{1,0:T(8,128)(2,1)S(1)} %get-tuple-element.24), channel_id=1, source_target_pairs={{0,1},{1,0},{2,3},{3,2},{4,5},{5,4},{6,7},{7,6},{8,9},{9,8},{10,11... | collective-permute-start | bytes 147464 | tf_op jit(solution)/shard_map/ppermute | solution.py:208
